TPU v7x, 32 devices: a whole 2x2x4 slice. The times are simulated.
32 devices in a mesh: sp: 8 (over z, y), dp: 4 (over x, core).
Axes of the slice: x: 2, y: 2, z: 4, core: 2. Of those that a mesh axis runs over, the one named last changes fastest.
Arguments:
- hidden_in: bfloat16 [4, 1024, 2048], P('dp', 'sp'), may hold values from -6 to 6
- queries: bfloat16 [4, 1024, 1536], P('dp', 'sp'), may hold values from -64 to 64
- key_value_latent: bfloat16 [4, 1024, 512], P('dp', 'sp'), may hold values from -6 to 6
- keys_rope: bfloat16 [4, 1024, 32], P('dp', 'sp'), may hold values from -4 to 4
- latent_norm_gain: float32 [512], replicated, may hold values from 0.1 to 1.9
- latent_up_weight: bfloat16 [512, 2048], replicated, may hold values from -0.25 to 0.25
- attn_gain: float32 [1024], replicated, may hold values from 0.1 to 1.9
- out_proj: bfloat16 [1024, 2048], replicated, may hold values from -0.1875 to 0.1875
- norm1_gain: float32 [2048], replicated, may hold values from 0.1 to 1.9
- norm1_bias: float32 [2048], replicated, may hold values from -1.5 to 1.5
- expert_ids: int32 [4, 1024, 4], P('dp', 'sp'), may hold values from 0 to 31, all different within a row; in each aligned block of 128 rows (0 to 127, 128 to 255, ..., all dimensions but the last counted through in order) at most 24 rows name the same one
- route_weights: float32 [4, 1024, 4], P('dp', 'sp'), may hold values from 0.1 to 1
- gate_proj: bfloat16 [32, 2048, 512], P(('sp', 'dp')), may hold values from -0.125 to 0.125
- up_proj: bfloat16 [32, 2048, 512], P(('sp', 'dp')), may hold values from -0.125 to 0.125
- down_proj: bfloat16 [32, 512, 2048], P(('sp', 'dp')), may hold values from -0.25 to 0.25
- shared_gate: bfloat16 [2048, 512], replicated, may hold values from -0.125 to 0.125
- shared_up: bfloat16 [2048, 512], replicated, may hold values from -0.125 to 0.125
- shared_down: bfloat16 [512, 2048], replicated, may hold values from -0.25 to 0.25
- norm2_gain: float32 [2048], replicated, may hold values from 0.1 to 1.9
- norm2_bias: float32 [2048], replicated, may hold values from -1.5 to 1.5
Outputs:
- result: bfloat16 [4, 1024, 2048], P('dp', 'sp')
Inputs may be any that keep to these rules, and one draw needn't show every extreme that they name: `expert_ids`: each row names 4 different experts. Among the rows of one device (aligned blocks of 128 rows), no expert is named more than 24 times, a bound that some block reaches.
All inputs are finite; a program needn't handle non-finite values.
Results may differ from a plain program's by a relative error of at most 0.01.
Values may be sent and summed in bfloat16 or wider, within the bound.
No kernel may reach another device: no remote copies, remote signals or barrier semaphores. Data moves between devices by JAX's collectives and lax.ppermute only.
A program may use at most 128 MiB of HBM per device.

v0:
```python
import functools
import math

import jax
import jax.numpy as jnp
import numpy as np
from jax import lax
from jax.experimental import pallas as pl
from jax.experimental.pallas import tpu as pltpu
from jax.sharding import PartitionSpec as P


D = 2048
PLAIN_HEAD_WIDTH = 64
QK_ROPE = 32
VALUE_HEAD_WIDTH = 64
TOP_K = 4


ALPHA = 2.0**0.25
ROUTED = 2.5
THETA = 10000.0
LANES = 128
MASKED = -1e30
ROPE_LANE = 64
TAG_LANE = ROPE_LANE + QK_ROPE
HEADS_STEP = 4
VMEM_LIMIT = 32 << 20
VMEM_WIDE = 60 << 20


def rms_scaled(values, scaling):
    widened = values.astype(jnp.float32)
    return (
        widened * lax.rsqrt(jnp.mean(widened * widened, axis=-1, keepdims=True) + 1e-06) * scaling
    )


def layer_norm(values, scaling, bias_add):
    centre = values - jnp.mean(values, axis=-1, keepdims=True)
    spread = jnp.mean(centre * centre, axis=-1, keepdims=True)
    return centre * lax.rsqrt(spread + 1e-05) * scaling + bias_add


def rotation_table(positions, rot_width):
    frequency = np.float32(THETA) ** (-np.arange(0, rot_width, 2, dtype=np.float32) / rot_width)
    angles = np.arange(positions, dtype=np.float32)[:, None] * frequency[None, :]
    table = np.zeros((positions, LANES), np.float32)
    half = rot_width // 2
    for side, values in enumerate((np.cos(angles), np.sin(angles))):
        start = ROPE_LANE + side * rot_width
        table[:, start : start + rot_width] = np.concatenate([values, values], axis=1)
    table[:, ROPE_LANE + rot_width : ROPE_LANE + rot_width + half] *= -1.0
    return jnp.asarray(table)


def turned(tile, table):
    lane = lax.broadcasted_iota(jnp.int32, tile.shape, 1)
    inside = (lane >= ROPE_LANE) & (lane < ROPE_LANE + QK_ROPE)
    half = QK_ROPE // 2
    other = jnp.where(
        lane < ROPE_LANE + half, pltpu.roll(tile, LANES - half, 1), pltpu.roll(tile, half, 1)
    )
    return jnp.where(inside, tile * table + other * pltpu.roll(table, LANES - QK_ROPE, 1), 0.0)


def pack_kernel(
    here_ref, latent_ref, gain_ref, rope_ref, ids_ref, weights_ref, table_ref, out_ref
):
    width = latent_ref.shape[1]
    rows = latent_ref.shape[0]
    out_ref[:, :width] = rms_scaled(latent_ref[...], gain_ref[...]).astype(jnp.bfloat16)
    weights = weights_ref[...]
    gates = weights / jnp.sum(weights, axis=0, keepdims=True) * ROUTED
    side = jnp.concatenate(
        [
            jnp.zeros((ROPE_LANE, rows), jnp.float32),
            rope_ref[...].astype(jnp.float32),
            ids_ref[...].astype(jnp.float32),
            gates,
            jnp.zeros((LANES - TAG_LANE - 2 * TOP_K, rows), jnp.float32),
        ],
        axis=0,
    ).T
    lane = lax.broadcasted_iota(jnp.int32, side.shape, 1)
    inside = (lane >= ROPE_LANE) & (lane < ROPE_LANE + QK_ROPE)
    out_ref[:, width:] = jnp.where(inside, turned(side, table_ref[...]), side).astype(
        jnp.bfloat16
    )


def pack(here, latent, gain, rope, ids, weights, table):
    rows, width = latent.shape
    whole = lambda array: pl.BlockSpec(array.shape, lambda i, here: (0,) * array.ndim)
    return pl.pallas_call(
        pack_kernel,
        grid_spec=pltpu.PrefetchScalarGridSpec(
            num_scalar_prefetch=1,
            grid=(1,),
            in_specs=[
                whole(latent),
                whole(gain),
                whole(rope),
                whole(ids),
                whole(weights),
                pl.BlockSpec((rows, LANES), lambda i, here: (here[0], 0)),
            ],
            out_specs=pl.BlockSpec((rows, width + LANES), lambda i, here: (0, 0)),
        ),
        out_shape=jax.ShapeDtypeStruct((rows, width + LANES), jnp.bfloat16),
        compiler_params=pltpu.CompilerParams(vmem_limit_bytes=VMEM_WIDE),
        name="pack",
    )(here, latent, gain, rope, ids, weights, table)


def pick_kernel(picks_ref, own_ref, other_ref, *out_refs):
    both = jnp.concatenate([own_ref[...], other_ref[...]], axis=0)
    sent = jnp.dot(picks_ref[...], both, preferred_element_type=jnp.float32).astype(jnp.bfloat16)
    step = out_refs[0].shape[0]
    for o, out_ref in enumerate(out_refs):
        out_ref[...] = sent[o * step : (o + 1) * step, :]


def pick(picks, own, other, peers):
    rows, width = picks.shape[0] // peers, own.shape[1]
    return pl.pallas_call(
        pick_kernel,
        out_shape=[jax.ShapeDtypeStruct((rows, width), jnp.bfloat16)] * peers,
        compiler_params=pltpu.CompilerParams(vmem_limit_bytes=VMEM_LIMIT),
        name="pick",
    )(picks, own, other)


def mix_kernel(mixes_ref, *refs):
    parts, (own_ref, other_ref) = refs[:-2], refs[-2:]
    whole = jnp.concatenate([p[...] for p in parts], axis=0)
    mixed = jnp.dot(mixes_ref[...], whole, preferred_element_type=jnp.float32)
    rows = own_ref.shape[0]
    own_ref[...] = mixed[:rows]
    other_ref[...] = mixed[rows:].astype(jnp.bfloat16)


def mix(mixes, parts):
    shape = (mixes.shape[0] // 2, parts[0].shape[1])
    return pl.pallas_call(
        mix_kernel,
        out_shape=[
            jax.ShapeDtypeStruct(shape, jnp.float32),
            jax.ShapeDtypeStruct(shape, jnp.bfloat16),
        ],
        compiler_params=pltpu.CompilerParams(vmem_limit_bytes=VMEM_LIMIT),
        name="mix",
    )(mixes, *parts)


def swiglu_kernel(count, after, scale, *refs):
    parts = refs[:count]
    gate_ref, up_ref, down_ref = refs[count : count + 3]
    outs, (held, total) = refs[count + 3 + after : -2], refs[-2:]
    step = pl.program_id(0)
    size = parts[0].shape[0]

    @pl.when(step == 0)
    def _():
        for o, part in enumerate(parts):
            held[o * size : (o + 1) * size, :] = part[...]
        if scale:
            total[...] = scale * held[...].astype(jnp.float32)
        else:
            total[...] = jnp.zeros_like(total)

    rows = held[...]
    gated = jnp.dot(rows, gate_ref[...], preferred_element_type=jnp.float32)
    lifted = jnp.dot(rows, up_ref[...], preferred_element_type=jnp.float32)
    inner = (gated / (1.0 + jnp.exp(-gated)) * lifted).astype(jnp.bfloat16)
    total[...] += jnp.dot(inner, down_ref[...], preferred_element_type=jnp.float32)

    @pl.when(step == pl.num_programs(0) - 1)
    def _():
        for o, out in enumerate(outs):
            out[...] = total[o * size : (o + 1) * size, :].astype(out.dtype)


def swiglu(parts, gate_mat, up_mat, down_mat, kind, after=(), scale=0.0):
    count, (size, width) = len(parts), parts[0].shape
    hidden = gate_mat.shape[-1]
    block = min(hidden, 256)
    lead = (None,) * (gate_mat.ndim - 2)
    zero = (0,) * len(lead)
    whole = pl.BlockSpec((size, width), lambda i: (0, 0))
    return pl.pallas_call(
        functools.partial(swiglu_kernel, count, len(after), scale),
        grid=(hidden // block,),
        in_specs=[whole] * count
        + [pl.BlockSpec((*lead, width, block), lambda i: (*zero, 0, i))] * 2
        + [pl.BlockSpec((*lead, block, width), lambda i: (*zero, i, 0))]
        + [pl.BlockSpec(memory_space=pl.ANY)] * len(after),
        out_specs=[whole] * count,
        out_shape=[jax.ShapeDtypeStruct((size, width), kind)] * count,
        scratch_shapes=[
            pltpu.VMEM((count * size, width), jnp.bfloat16),
            pltpu.VMEM((count * size, width), jnp.float32),
        ],
        compiler_params=pltpu.CompilerParams(
            dimension_semantics=("arbitrary",), vmem_limit_bytes=VMEM_LIMIT
        ),
        name="swiglu",
    )(*parts, gate_mat, up_mat, down_mat, *after)


def finish_kernel(feed_ref, own_ref, core_ref, far_ref, gain_ref, bias_ref, out_ref):
    feed = feed_ref[...] + own_ref[...] + core_ref[...].astype(jnp.float32)
    feed = feed + far_ref[...].astype(jnp.float32)
    out_ref[...] = layer_norm(feed, gain_ref[...], bias_ref[...]).astype(jnp.bfloat16)


def finish(feed, *args):
    return pl.pallas_call(
        finish_kernel,
        out_shape=jax.ShapeDtypeStruct(feed.shape, jnp.bfloat16),
        compiler_params=pltpu.CompilerParams(vmem_limit_bytes=VMEM_LIMIT),
        name="finish",
    )(feed, *args)


def depth_of(seq_devices):
    bits = seq_devices.bit_length() - 1
    return 1 << ((bits + 1) // 2)


def send(values, dsp, ddp):
    count, side = lax.axis_size("sp"), lax.axis_size("dp")
    pairs = [
        (i * side + k, (i ^ dsp) * side + (k ^ ddp)) for i in range(count) for k in range(side)
    ]
    return lax.ppermute(values, ("sp", "dp"), pairs)


def attention_kernel(blocks, after, latent_width, here_ref, query_ref, table_ref, *refs):
    packed_refs = refs[:blocks]
    (
        up_ref,
        hidden_ref,
        attn_gain_ref,
        gain_ref,
        bias_ref,
        out_proj_ref,
    ) = refs[blocks : blocks + 6]
    out_ref, latent, rope, attended, out_proj, sem = refs[blocks + 6 + after :]
    step = pl.program_id(0)
    steps = pl.num_programs(0)
    rows = hidden_ref.shape[0]
    load = pltpu.make_async_copy(out_proj_ref, out_proj, sem)

    @pl.when(step == 0)
    def _():
        load.start()
        for j in range(blocks):
            latent[j * rows : (j + 1) * rows, :] = packed_refs[j][:, :latent_width]
            rope[j * rows : (j + 1) * rows, :] = packed_refs[j][:, latent_width:]

    key_values = jnp.dot(latent[...], up_ref[...], preferred_element_type=jnp.float32).astype(
        jnp.bfloat16
    )
    here = here_ref[0]
    width = PLAIN_HEAD_WIDTH + VALUE_HEAD_WIDTH
    key_width = PLAIN_HEAD_WIDTH + QK_ROPE
    factor = math.log2(math.e) / math.sqrt(key_width)
    causal = lax.broadcasted_iota(jnp.int32, (rows, rows), 1) <= lax.broadcasted_iota(
        jnp.int32, (rows, rows), 0
    )
    lane = lax.broadcasted_iota(jnp.int32, (rows, LANES), 1)
    query = query_ref[...].astype(jnp.float32)
    outs = []
    for head in range(HEADS_STEP):
        tile, offset = divmod(head * key_width, LANES)
        mine = query[:, tile * LANES : (tile + 1) * LANES]
        if offset:
            mine = pltpu.roll(mine, LANES - offset, 1)
        if offset + key_width > LANES:
            after = query[:, (tile + 1) * LANES : (tile + 2) * LANES]
            mine = jnp.where(lane < LANES - offset, mine, pltpu.roll(after, LANES - offset, 1))
        query_full = jnp.concatenate(
            [jnp.where(lane < PLAIN_HEAD_WIDTH, mine, 0.0), turned(mine, table_ref[...])], axis=1
        ).astype(jnp.bfloat16)
        head_kv = key_values[:, head * width : (head + 1) * width]
        key_full = jnp.concatenate([head_kv, rope[...]], axis=1)
        scores = lax.dot_general(
            query_full,
            key_full,
            (((1,), (1,)), ((), ())),
            preferred_element_type=jnp.float32,
        )
        parts = [jnp.where(causal, scores[:, :rows], MASKED)]
        for j in range(1, blocks):
            seen = (here ^ j) < here
            parts.append(jnp.where(seen, scores[:, j * rows : (j + 1) * rows], MASKED))
        scores = jnp.concatenate(parts, axis=1)
        row_max = jnp.max(scores, axis=1, keepdims=True)
        weights = jnp.exp2((scores - row_max) * factor)
        total = jnp.sum(weights, axis=1, keepdims=True)
        summed = jnp.dot(
            weights.astype(jnp.bfloat16), head_kv, preferred_element_type=jnp.float32
        )
        outs.append(summed / total)
    for pair in range(HEADS_STEP // 2):
        left, right = outs[2 * pair : 2 * pair + 2]
        attended[step * (HEADS_STEP // 2) + pair] = jnp.where(
            lane < VALUE_HEAD_WIDTH, pltpu.roll(left, VALUE_HEAD_WIDTH, 1), right
        ).astype(jnp.bfloat16)

    @pl.when(step == steps - 1)
    def _():
        load.wait()
        whole = jnp.concatenate([attended[i] for i in range(attended.shape[0])], axis=1)
        normed = rms_scaled(whole, attn_gain_ref[...]).astype(jnp.bfloat16)
        mixed = jnp.dot(normed, out_proj[...], preferred_element_type=jnp.float32)
        out_ref[...] = layer_norm(
            ALPHA * hidden_ref[...].astype(jnp.float32) + mixed, gain_ref[...], bias_ref[...]
        ).astype(jnp.bfloat16)


def attention_layer(
    here, queries, table, packed, latent_up_weight, hidden, attn_gain, out_proj, gain, bias, after=()
):
    blocks = len(packed)
    rows = queries.shape[0]
    latent_width = latent_up_weight.shape[0]
    width = PLAIN_HEAD_WIDTH + VALUE_HEAD_WIDTH
    heads = latent_up_weight.shape[1] // width
    whole = lambda array: pl.BlockSpec(array.shape, lambda i, here: (0,) * array.ndim)
    return pl.pallas_call(
        functools.partial(attention_kernel, blocks, len(after), latent_width),
        grid_spec=pltpu.PrefetchScalarGridSpec(
            num_scalar_prefetch=1,
            grid=(heads // HEADS_STEP,),
            in_specs=[
                pl.BlockSpec(
                    (rows, HEADS_STEP * (PLAIN_HEAD_WIDTH + QK_ROPE)), lambda i, here: (0, i)
                ),
                pl.BlockSpec((rows, LANES), lambda i, here: (here[0], 0)),
                *[whole(p) for p in packed],
                pl.BlockSpec((latent_width, HEADS_STEP * width), lambda i, here: (0, i)),
                whole(hidden),
                whole(attn_gain),
                whole(gain),
                whole(bias),
                pl.BlockSpec(memory_space=pltpu.HBM),
                *[pl.BlockSpec(memory_space=pl.ANY)] * len(after),
            ],
            out_specs=pl.BlockSpec(hidden.shape, lambda i, here: (0, 0)),
            scratch_shapes=[
                pltpu.VMEM((blocks * rows, latent_width), jnp.bfloat16),
                pltpu.VMEM((blocks * rows, LANES), jnp.bfloat16),
                pltpu.VMEM((heads // 2, rows, 2 * VALUE_HEAD_WIDTH), jnp.bfloat16),
                pltpu.VMEM(out_proj.shape, jnp.bfloat16),
                pltpu.SemaphoreType.DMA,
            ],
        ),
        out_shape=jax.ShapeDtypeStruct(hidden.shape, jnp.bfloat16),
        compiler_params=pltpu.CompilerParams(
            dimension_semantics=("arbitrary",), vmem_limit_bytes=VMEM_WIDE
        ),
        name="attention_layer",
    )(here, queries, table, *packed, latent_up_weight, hidden, attn_gain, gain, bias, out_proj, *after)


def per_device(
    hidden_in,
    queries,
    key_value_latent,
    keys_rope,
    latent_norm_gain,
    latent_up_weight,
    attn_gain,
    out_proj,
    norm1_gain,
    norm1_bias,
    expert_ids,
    route_weights,
    gate_proj,
    up_proj,
    down_proj,
    shared_gate,
    shared_up,
    shared_down,
    norm2_gain,
    norm2_bias,
):
    seq_devices = lax.axis_size("sp")
    depth = depth_of(seq_devices)
    across = seq_devices // depth
    tok_rows = hidden_in.shape[1]
    here = lax.axis_index("sp")

    index = here.reshape(1).astype(jnp.int32)
    table = rotation_table(seq_devices * tok_rows, QK_ROPE)

    packed = pack(
        index,
        key_value_latent[0],
        latent_norm_gain[None],
        keys_rope[0].T,
        expert_ids[0].T,
        route_weights[0].T,
        table,
    )
    gathered = [packed] + [None] * (seq_devices - 1)
    for dz in range(depth - 1, 0, -1):
        gathered[dz * across] = send(packed, dz * across, 0)
    for dy in range(1, across):
        gathered[dy] = send(packed, dy, 0)
    for dz in range(1, depth):
        for dy in range(1, across):
            gathered[dz * across + dy] = send(gathered[dz * across], dy, 0)

    side_devices = lax.axis_size("dp")
    group = seq_devices * side_devices
    capacity = (tok_rows * TOP_K * 3 + 2 * group - 1) // (2 * group)
    capacity = -(-capacity // 8) * 8
    half = seq_devices // 2
    offsets = [(d, k) for d in range(half) for k in range(0, side_devices, 2)]
    offsets = offsets[:1] + offsets[:0:-1]
    peers = len(offsets)
    slots = peers * 2 * capacity
    column = lax.axis_index("dp")
    wanted = jnp.stack([(here ^ d) * side_devices + (column ^ k) for d, k in offsets]).astype(
        jnp.float32
    )
    order = jnp.arange(tok_rows)
    before = (order[:, None] > order[None, :]).astype(jnp.bfloat16)
    same = jnp.eye(2, dtype=jnp.bool_)
    start = key_value_latent.shape[2] + TAG_LANE

    def routes(block):
        tags = block[:, start : start + 2 * TOP_K]
        tags = jnp.stack([tags, send(tags, 0, 1)]).astype(jnp.float32)
        named = tags[..., :TOP_K, None] == wanted
        member = jnp.any(named, axis=2)
        share = jnp.sum(jnp.where(named, tags[..., TOP_K:, None], 0.0), axis=2)
        slot = jnp.einsum(
            "ts,bsp->btp", before, member.astype(jnp.bfloat16), preferred_element_type=jnp.float32
        ).astype(jnp.int32)
        filled = member[..., None] & (slot[..., None] == jnp.arange(capacity, dtype=jnp.int32))
        picks = (
            (jnp.transpose(filled, (2, 0, 3, 1))[:, :, :, None, :] & same[:, None, :, None])
            .reshape(slots, 2 * tok_rows)
            .astype(jnp.bfloat16)
        )
        gated = jnp.where(filled, share[..., None], 0.0)
        mixes = (
            jnp.where(same[:, None, None, :, None], gated[:, :, :, None, :], 0.0)
            .reshape(2 * tok_rows, slots)
            .astype(jnp.bfloat16)
        )
        return picks, mixes

    near_picks, near_mixes = routes(packed)
    far_picks, far_mixes = routes(gathered[half])

    first = attention_layer(
        index,
        queries[0],
        table,
        gathered,
        latent_up_weight,
        hidden_in[0],
        attn_gain[None],
        out_proj,
        norm1_gain[None],
        norm1_bias[None],
        (near_picks, far_picks, near_mixes, far_mixes),
    )

    def exchange(parts):
        return [parts[0]] + [send(parts[o], *offsets[o]) for o in range(1, peers)]

    experts = functools.partial(swiglu, gate_mat=gate_proj, up_mat=up_proj, down_mat=down_proj)
    far = send(first, half, 0)
    sibling = send(first, 0, 1)
    near_sent = pick(near_picks, first, sibling, peers)
    near = exchange(near_sent)
    (feed,) = swiglu(
        [first], shared_gate, shared_up, shared_down, jnp.float32, near_sent[:1], ALPHA
    )
    far_sibling = send(far, 0, 1)
    far_sent = pick(far_picks, far, far_sibling, peers)
    away = exchange(far_sent)
    near_done = experts(near, kind=jnp.bfloat16, after=(far_sent[1], feed))
    away_done = experts(away, kind=jnp.bfloat16, after=near_done[1:2])
    away_back = exchange(away_done)
    near_back = exchange(near_done)
    far_own, far_core = mix(far_mixes, away_back)
    far_core = send(far_core, 0, 1)
    far_sum = (far_own + far_core.astype(jnp.float32)).astype(jnp.bfloat16)
    far_sum = send(far_sum, half, 0)
    own, core = mix(near_mixes, near_back)
    core = send(core, 0, 1)
    result = finish(feed, own, core, far_sum, norm2_gain[None], norm2_bias[None])
    return result.reshape(1, tok_rows, D)


def solution(mesh):
    in_specs = (
        P("dp", "sp", None),
        P("dp", "sp", None),
        P("dp", "sp", None),
        P("dp", "sp", None),
        P(),
        P(),
        P(),
        P(),
        P(),
        P(),
        P("dp", "sp", None),
        P("dp", "sp", None),
        P(("sp", "dp"), None, None),
        P(("sp", "dp"), None, None),
        P(("sp", "dp"), None, None),
        P(),
        P(),
        P(),
        P(),
        P(),
    )
    out_specs = P("dp", "sp", None)
    return jax.shard_map(
        per_device, mesh=mesh, in_specs=in_specs, out_specs=out_specs, check_vma=False
    )
```

profile of v0, /device:TPU:0, one launch (start us, length us, event | category | flops | bytes accessed | tf_op | source)
XLA Modules:
  0.0 198.4 jit_solution(9345881120448372446)
XLA Ops:
  1.9 4.1 %collective-permute-start.3 = (bf16[128,640]{1,0:T(8,128)(2,1)}, bf16[128,640]{1,0:T(8,128)(2,1)S(1)}, u32[]{:S(2)}, u32[]{:S(2)}) collective-permute-start(bf16[128,640]{1,0:T(8,128)(2,1)} %pack.1.refs_0_), channel_id=1, source_target_pairs={{0,16},{1,17},{2,18},{3,19},{4,20},{5,21},{6,22},{7,23},{8,24},{9,... | collective-permute-start | bytes 491528 | tf_op jit(solution)/shard_map/ppermute | solution.py:236
  11.4 4.1 %collective-permute-done.3.refs_4_ = bf16[128,640]{1,0:T(8,128)(2,1)S(1)} collective-permute-done((bf16[128,640]{1,0:T(8,128)(2,1)}, bf16[128,640]{1,0:T(8,128)(2,1)S(1)}, u32[]{:S(2)}, u32[]{:S(2)}) %collective-permute-start.3) | collective-permute-done | bytes 163872 | tf_op jit(solution)/shard_map/ppermute | solution.py:236
  15.7 2.1 %collective-permute-start.4 = (bf16[128,640]{1,0:T(8,128)(2,1)S(1)}, bf16[128,640]{1,0:T(8,128)(2,1)S(1)}, u32[]{:S(2)}, u32[]{:S(2)}) collective-permute-start(bf16[128,640]{1,0:T(8,128)(2,1)S(1)} %collective-permute-done.3.refs_4_), channel_id=1, source_target_pairs={{0,4},{1,5},{2,6},{3,7},{4,0},{5,1},{6,2},{7,3},{8,12},{9,13},{10,... | collective-permute-start | bytes 491528 | tf_op jit(solution)/shard_map/ppermute | solution.py:236
  26.4 3.3 %collective-permute-done.6.refs_7_ = bf16[128,640]{1,0:T(8,128)(2,1)S(1)} collective-permute-done((bf16[128,640]{1,0:T(8,128)(2,1)S(1)}, bf16[128,640]{1,0:T(8,128)(2,1)S(1)}, u32[]{:S(2)}, u32[]{:S(2)}) %collective-permute-start.6) | collective-permute-done | bytes 163872 | tf_op jit(solution)/shard_map/ppermute | solution.py:236
  30.4 14.2 %attention_layer.1.own_ref.refs_0_ = bf16[128,2048]{1,0:T(8,128)(2,1)} custom-call(s32[1]{0:T(128)} %bitcast.here_ref, bf16[128,1536]{1,0:T(8,128)(2,1)} %bitcast.83, f32[1024,128]{1,0:T(8,128)} %constant.23.clone.table_ref, bf16[128,640]{1,0:T(8,128)(2,1)} %pack.1.refs_0_, bf16[128,640]{1,0:T(8,128)(2,1)} %copy-done.17, bf16[128,640]{1,0:T(8,128)(2,1)} %copy-done.15, ...), custom_call_target="tpu_custom_call" | custom-call | tf_op jit(solution)/shard_map/attention_layer/pallas_call | solution.py:332
  45.3 25.3 %collective-permute-done.17.own_ref = bf16[128,2048]{1,0:T(8,128)(2,1)S(1)} collective-permute-done((bf16[128,2048]{1,0:T(8,128)(2,1)}, bf16[128,2048]{1,0:T(8,128)(2,1)S(1)}, u32[]{:S(2)}, u32[]{:S(2)}) %collective-permute-start.17) | collective-permute-done | bytes 524320 | tf_op jit(solution)/shard_map/ppermute | solution.py:236
  72.8 3.4 %collective-permute-start.11 = (bf16[48,2048]{1,0:T(8,128)(2,1)S(1)}, bf16[48,2048]{1,0:T(8,128)(2,1)S(1)}, u32[]{:S(2)}, u32[]{:S(2)}) collective-permute-start(bf16[48,2048]{1,0:T(8,128)(2,1)S(1)} %get-tuple-element.43), channel_id=1, source_target_pairs={{0,12},{1,13},{2,14},{3,15},{4,8},{5,9},{6,10},{7,11},{8,4},{9,5},... | collective-permute-start | bytes 589832 | tf_op jit(solution)/shard_map/ppermute | solution.py:236
  78.2 2.5 %collective-permute-start.14 = (bf16[48,2048]{1,0:T(8,128)(2,1)S(1)}, bf16[48,2048]{1,0:T(8,128)(2,1)S(1)}, u32[]{:S(2)}, u32[]{:S(2)}) collective-permute-start(bf16[48,2048]{1,0:T(8,128)(2,1)S(1)} %get-tuple-element.46), channel_id=1, source_target_pairs={{0,6},{1,7},{2,4},{3,5},{4,2},{5,3},{6,0},{7,1},{8,14},{9,15},{10,... | collective-permute-start | bytes 589832 | tf_op jit(solution)/shard_map/ppermute | solution.py:236
  83.8 6.0 %collective-permute-done.11.refs_2_ = bf16[48,2048]{1,0:T(8,128)(2,1)S(1)} collective-permute-done((bf16[48,2048]{1,0:T(8,128)(2,1)S(1)}, bf16[48,2048]{1,0:T(8,128)(2,1)S(1)}, u32[]{:S(2)}, u32[]{:S(2)}) %collective-permute-start.11) | collective-permute-done | bytes 196640 | tf_op jit(solution)/shard_map/ppermute | solution.py:236
  90.4 2.7 %collective-permute-done.12.refs_3_ = bf16[48,2048]{1,0:T(8,128)(2,1)S(1)} collective-permute-done((bf16[48,2048]{1,0:T(8,128)(2,1)S(1)}, bf16[48,2048]{1,0:T(8,128)(2,1)S(1)}, u32[]{:S(2)}, u32[]{:S(2)}) %collective-permute-start.12) | collective-permute-done | bytes 196640 | tf_op jit(solution)/shard_map/ppermute | solution.py:236
  93.5 3.9 %collective-permute-done.13.refs_4_ = bf16[48,2048]{1,0:T(8,128)(2,1)S(1)} collective-permute-done((bf16[48,2048]{1,0:T(8,128)(2,1)S(1)}, bf16[48,2048]{1,0:T(8,128)(2,1)S(1)}, u32[]{:S(2)}, u32[]{:S(2)}) %collective-permute-start.13) | collective-permute-done | bytes 196640 | tf_op jit(solution)/shard_map/ppermute | solution.py:236
  104.4 4.4 %collective-permute-done.28.refs_2_ = bf16[48,2048]{1,0:T(8,128)(2,1)S(1)} collective-permute-done((bf16[48,2048]{1,0:T(8,128)(2,1)S(1)}, bf16[48,2048]{1,0:T(8,128)(2,1)S(1)}, u32[]{:S(2)}, u32[]{:S(2)}) %collective-permute-start.28) | collective-permute-done | bytes 196640 | tf_op jit(solution)/shard_map/ppermute | solution.py:236
  115.6 3.7 %swiglu.4 = (bf16[48,2048]{1,0:T(8,128)(2,1)S(1)}, bf16[48,2048]{1,0:T(8,128)(2,1)S(1)}, bf16[48,2048]{1,0:T(8,128)(2,1)S(1)}, bf16[48,2048]{1,0:T(8,128)(2,1)S(...) custom-call(bf16[48,2048]{1,0:T(8,128)(2,1)S(1)} %get-tuple-element., ...), custom_call_target="tpu_custom_call" | custom-call | tf_op jit(solution)/shard_map/swiglu/pallas_call | solution.py:191
  119.4 4.0 %swiglu.5 = (bf16[48,2048]{1,0:T(8,128)(2,1)S(1)}, bf16[48,2048]{1,0:T(8,128)(2,1)S(1)}, bf16[48,2048]{1,0:T(8,128)(2,1)S(1)}, bf16[48,2048]{1,0:T(8,128)(2,1)S(...) custom-call(bf16[48,2048]{1,0:T(8,128)(2,1)S(1)} %get-tuple-element., ...), custom_call_target="tpu_custom_call" | custom-call | tf_op jit(solution)/shard_map/swiglu/pallas_call | solution.py:191
  123.5 3.6 %collective-permute-start.35 = (bf16[48,2048]{1,0:T(8,128)(2,1)S(1)}, bf16[48,2048]{1,0:T(8,128)(2,1)S(1)}, u32[]{:S(2)}, u32[]{:S(2)}) collective-permute-start(bf16[48,2048]{1,0:T(8,128)(2,1)S(1)} %get-tuple-element.69), channel_id=1, source_target_pairs={{0,12},{1,13},{2,14},{3,15},{4,8},{5,9},{6,10},{7,11},{8,4},{9,5},... | collective-permute-start | bytes 589832 | tf_op jit(solution)/shard_map/ppermute | solution.py:236
  129.3 2.5 %collective-permute-start.38 = (bf16[48,2048]{1,0:T(8,128)(2,1)S(1)}, bf16[48,2048]{1,0:T(8,128)(2,1)S(1)}, u32[]{:S(2)}, u32[]{:S(2)}) collective-permute-start(bf16[48,2048]{1,0:T(8,128)(2,1)S(1)} %get-tuple-element.72), channel_id=1, source_target_pairs={{0,6},{1,7},{2,4},{3,5},{4,2},{5,3},{6,0},{7,1},{8,14},{9,15},{10,... | collective-permute-start | bytes 589832 | tf_op jit(solution)/shard_map/ppermute | solution.py:236
  135.0 2.9 %collective-permute-done.35.refs_2_ = bf16[48,2048]{1,0:T(8,128)(2,1)S(1)} collective-permute-done((bf16[48,2048]{1,0:T(8,128)(2,1)S(1)}, bf16[48,2048]{1,0:T(8,128)(2,1)S(1)}, u32[]{:S(2)}, u32[]{:S(2)}) %collective-permute-start.35) | collective-permute-done | bytes 196640 | tf_op jit(solution)/shard_map/ppermute | solution.py:236
  138.5 2.8 %collective-permute-done.36.refs_3_ = bf16[48,2048]{1,0:T(8,128)(2,1)S(1)} collective-permute-done((bf16[48,2048]{1,0:T(8,128)(2,1)S(1)}, bf16[48,2048]{1,0:T(8,128)(2,1)S(1)}, u32[]{:S(2)}, u32[]{:S(2)}) %collective-permute-start.36) | collective-permute-done | bytes 196640 | tf_op jit(solution)/shard_map/ppermute | solution.py:236
  146.8 2.9 %collective-permute-start.20 = (bf16[48,2048]{1,0:T(8,128)(2,1)S(1)}, bf16[48,2048]{1,0:T(8,128)(2,1)S(1)}, u32[]{:S(2)}, u32[]{:S(2)}) collective-permute-start(bf16[48,2048]{1,0:T(8,128)(2,1)S(1)} %get-tuple-element.52), channel_id=1, source_target_pairs={{0,12},{1,13},{2,14},{3,15},{4,8},{5,9},{6,10},{7,11},{8,4},{9,5},... | collective-permute-start | bytes 589832 | tf_op jit(solution)/shard_map/ppermute | solution.py:236
  151.8 3.8 %collective-permute-done.19.refs_1_ = bf16[48,2048]{1,0:T(8,128)(2,1)S(1)} collective-permute-done((bf16[48,2048]{1,0:T(8,128)(2,1)S(1)}, bf16[48,2048]{1,0:T(8,128)(2,1)S(1)}, u32[]{:S(2)}, u32[]{:S(2)}) %collective-permute-start.19) | collective-permute-done | bytes 196640 | tf_op jit(solution)/shard_map/ppermute | solution.py:236
  157.1 3.4 %collective-permute-done.20.refs_2_ = bf16[48,2048]{1,0:T(8,128)(2,1)S(1)} collective-permute-done((bf16[48,2048]{1,0:T(8,128)(2,1)S(1)}, bf16[48,2048]{1,0:T(8,128)(2,1)S(1)}, u32[]{:S(2)}, u32[]{:S(2)}) %collective-permute-start.20) | collective-permute-done | bytes 196640 | tf_op jit(solution)/shard_map/ppermute | solution.py:236
  160.5 2.8 %collective-permute-done.21.refs_3_ = bf16[48,2048]{1,0:T(8,128)(2,1)S(1)} collective-permute-done((bf16[48,2048]{1,0:T(8,128)(2,1)S(1)}, bf16[48,2048]{1,0:T(8,128)(2,1)S(1)}, u32[]{:S(2)}, u32[]{:S(2)}) %collective-permute-start.21) | collective-permute-done | bytes 196640 | tf_op jit(solution)/shard_map/ppermute | solution.py:236
  164.0 2.2 %collective-permute-done.22.refs_4_ = bf16[48,2048]{1,0:T(8,128)(2,1)S(1)} collective-permute-done((bf16[48,2048]{1,0:T(8,128)(2,1)S(1)}, bf16[48,2048]{1,0:T(8,128)(2,1)S(1)}, u32[]{:S(2)}, u32[]{:S(2)}) %collective-permute-start.22) | collective-permute-done | bytes 196640 | tf_op jit(solution)/shard_map/ppermute | solution.py:236
  172.3 24.7 %collective-permute-done.42.far_ref = bf16[128,2048]{1,0:T(8,128)(2,1)S(1)} collective-permute-done((bf16[128,2048]{1,0:T(8,128)(2,1)S(1)}, bf16[128,2048]{1,0:T(8,128)(2,1)S(1)}, u32[]{:S(2)}, u32[]{:S(2)}) %collective-permute-start.42) | collective-permute-done | bytes 524320 | tf_op jit(solution)/shard_map/ppermute | solution.py:236
  (154 shorter events, 62.7 us)
Async XLA Ops:
  1.9 13.7 %collective-permute-start.3 = (bf16[128,640]{1,0:T(8,128)(2,1)}, bf16[128,640]{1,0:T(8,128)(2,1)S(1)}, u32[]{:S(2)}, u32[]{:S(2)}) collective-permute-start(bf16[128,640]{1,0:T(8,128)(2,1)} %pack.1.refs_0_), channel_id=1, source_target_pairs={{0,16},{1,17},{2,18},{3,19},{4,20},{5,21},{6,22},{7,23},{8,24},{9,... | collective-permute-start | bytes 491528 | tf_op jit(solution)/shard_map/ppermute | solution.py:236
  5.9 12.0 %collective-permute-start.1 = (bf16[128,640]{1,0:T(8,128)(2,1)}, bf16[128,640]{1,0:T(8,128)(2,1)S(1)}, u32[]{:S(2)}, u32[]{:S(2)}) collective-permute-start(bf16[128,640]{1,0:T(8,128)(2,1)} %pack.1.refs_0_), channel_id=1, source_target_pairs={{0,8},{1,9},{2,10},{3,11},{4,12},{5,13},{6,14},{7,15},{8,0},{9,1},... | collective-permute-start | bytes 491528 | tf_op jit(solution)/shard_map/ppermute | solution.py:236
  7.5 17.7 %collective-permute-start = (bf16[128,640]{1,0:T(8,128)(2,1)}, bf16[128,640]{1,0:T(8,128)(2,1)S(1)}, u32[]{:S(2)}, u32[]{:S(2)}) collective-permute-start(bf16[128,640]{1,0:T(8,128)(2,1)} %pack.1.refs_0_), channel_id=1, source_target_pairs={{0,4},{1,5},{2,6},{3,7},{4,0},{5,1},{6,2},{7,3},{8,12},{9,13},{10,... | collective-permute-start | bytes 491528 | tf_op jit(solution)/shard_map/ppermute | solution.py:236
  44.7 26.0 %collective-permute-start.17 = (bf16[128,2048]{1,0:T(8,128)(2,1)}, bf16[128,2048]{1,0:T(8,128)(2,1)S(1)}, u32[]{:S(2)}, u32[]{:S(2)}) collective-permute-start(bf16[128,2048]{1,0:T(8,128)(2,1)} %attention_layer.1.own_ref.refs_0_), channel_id=1, source_target_pairs={{0,16},{1,17},{2,18},{3,19},{4,20},{5,21},{6,22},{7,23},{8,24},{9,... | collective-permute-start | bytes 1572872 | tf_op jit(solution)/shard_map/ppermute | solution.py:236
  45.3 25.3 %collective-permute-start.9 = (bf16[128,2048]{1,0:T(8,128)(2,1)}, bf16[128,2048]{1,0:T(8,128)(2,1)S(1)}, u32[]{:S(2)}, u32[]{:S(2)}) collective-permute-start(bf16[128,2048]{1,0:T(8,128)(2,1)} %attention_layer.1.own_ref.refs_0_), channel_id=1, source_target_pairs={{0,1},{1,0},{2,3},{3,2},{4,5},{5,4},{6,7},{7,6},{8,9},{9,8},{10,11... | collective-permute-start | bytes 1572872 | tf_op jit(solution)/shard_map/ppermute | solution.py:236
  72.8 17.0 %collective-permute-start.11 = (bf16[48,2048]{1,0:T(8,128)(2,1)S(1)}, bf16[48,2048]{1,0:T(8,128)(2,1)S(1)}, u32[]{:S(2)}, u32[]{:S(2)}) collective-permute-start(bf16[48,2048]{1,0:T(8,128)(2,1)S(1)} %get-tuple-element.43), channel_id=1, source_target_pairs={{0,12},{1,13},{2,14},{3,15},{4,8},{5,9},{6,10},{7,11},{8,4},{9,5},... | collective-permute-start | bytes 589832 | tf_op jit(solution)/shard_map/ppermute | solution.py:236
  76.2 17.0 %collective-permute-start.12 = (bf16[48,2048]{1,0:T(8,128)(2,1)S(1)}, bf16[48,2048]{1,0:T(8,128)(2,1)S(1)}, u32[]{:S(2)}, u32[]{:S(2)}) collective-permute-start(bf16[48,2048]{1,0:T(8,128)(2,1)S(1)} %get-tuple-element.44), channel_id=1, source_target_pairs={{0,10},{1,11},{2,8},{3,9},{4,14},{5,15},{6,12},{7,13},{8,2},{9,3},... | collective-permute-start | bytes 589832 | tf_op jit(solution)/shard_map/ppermute | solution.py:236
  76.3 21.1 %collective-permute-start.13 = (bf16[48,2048]{1,0:T(8,128)(2,1)S(1)}, bf16[48,2048]{1,0:T(8,128)(2,1)S(1)}, u32[]{:S(2)}, u32[]{:S(2)}) collective-permute-start(bf16[48,2048]{1,0:T(8,128)(2,1)S(1)} %get-tuple-element.45), channel_id=1, source_target_pairs={{0,8},{1,9},{2,10},{3,11},{4,12},{5,13},{6,14},{7,15},{8,0},{9,1},... | collective-permute-start | bytes 589832 | tf_op jit(solution)/shard_map/ppermute | solution.py:236
  78.2 19.2 %collective-permute-start.14 = (bf16[48,2048]{1,0:T(8,128)(2,1)S(1)}, bf16[48,2048]{1,0:T(8,128)(2,1)S(1)}, u32[]{:S(2)}, u32[]{:S(2)}) collective-permute-start(bf16[48,2048]{1,0:T(8,128)(2,1)S(1)} %get-tuple-element.46), channel_id=1, source_target_pairs={{0,6},{1,7},{2,4},{3,5},{4,2},{5,3},{6,0},{7,1},{8,14},{9,15},{10,... | collective-permute-start | bytes 589832 | tf_op jit(solution)/shard_map/ppermute | solution.py:236
  82.3 16.7 %collective-permute-start.15 = (bf16[48,2048]{1,0:T(8,128)(2,1)S(1)}, bf16[48,2048]{1,0:T(8,128)(2,1)S(1)}, u32[]{:S(2)}, u32[]{:S(2)}) collective-permute-start(bf16[48,2048]{1,0:T(8,128)(2,1)S(1)} %get-tuple-element.47), channel_id=1, source_target_pairs={{0,4},{1,5},{2,6},{3,7},{4,0},{5,1},{6,2},{7,3},{8,12},{9,13},{10,... | collective-permute-start | bytes 589832 | tf_op jit(solution)/shard_map/ppermute | solution.py:236
  97.4 21.9 %collective-permute-start.29 = (bf16[48,2048]{1,0:T(8,128)(2,1)S(1)}, bf16[48,2048]{1,0:T(8,128)(2,1)S(1)}, u32[]{:S(2)}, u32[]{:S(2)}) collective-permute-start(bf16[48,2048]{1,0:T(8,128)(2,1)S(1)} %get-tuple-element.62), channel_id=1, source_target_pairs={{0,10},{1,11},{2,8},{3,9},{4,14},{5,15},{6,12},{7,13},{8,2},{9,3},... | collective-permute-start | bytes 589832 | tf_op jit(solution)/shard_map/ppermute | solution.py:236
  99.0 20.4 %collective-permute-start.30 = (bf16[48,2048]{1,0:T(8,128)(2,1)S(1)}, bf16[48,2048]{1,0:T(8,128)(2,1)S(1)}, u32[]{:S(2)}, u32[]{:S(2)}) collective-permute-start(bf16[48,2048]{1,0:T(8,128)(2,1)S(1)} %get-tuple-element.63), channel_id=1, source_target_pairs={{0,8},{1,9},{2,10},{3,11},{4,12},{5,13},{6,14},{7,15},{8,0},{9,1},... | collective-permute-start | bytes 589832 | tf_op jit(solution)/shard_map/ppermute | solution.py:236
  100.7 18.7 %collective-permute-start.31 = (bf16[48,2048]{1,0:T(8,128)(2,1)S(1)}, bf16[48,2048]{1,0:T(8,128)(2,1)S(1)}, u32[]{:S(2)}, u32[]{:S(2)}) collective-permute-start(bf16[48,2048]{1,0:T(8,128)(2,1)S(1)} %get-tuple-element.64), channel_id=1, source_target_pairs={{0,6},{1,7},{2,4},{3,5},{4,2},{5,3},{6,0},{7,1},{8,14},{9,15},{10,... | collective-permute-start | bytes 589832 | tf_op jit(solution)/shard_map/ppermute | solution.py:236
  102.5 16.9 %collective-permute-start.32 = (bf16[48,2048]{1,0:T(8,128)(2,1)S(1)}, bf16[48,2048]{1,0:T(8,128)(2,1)S(1)}, u32[]{:S(2)}, u32[]{:S(2)}) collective-permute-start(bf16[48,2048]{1,0:T(8,128)(2,1)S(1)} %get-tuple-element.65), channel_id=1, source_target_pairs={{0,4},{1,5},{2,6},{3,7},{4,0},{5,1},{6,2},{7,3},{8,12},{9,13},{10,... | collective-permute-start | bytes 589832 | tf_op jit(solution)/shard_map/ppermute | solution.py:236
  123.5 14.5 %collective-permute-start.35 = (bf16[48,2048]{1,0:T(8,128)(2,1)S(1)}, bf16[48,2048]{1,0:T(8,128)(2,1)S(1)}, u32[]{:S(2)}, u32[]{:S(2)}) collective-permute-start(bf16[48,2048]{1,0:T(8,128)(2,1)S(1)} %get-tuple-element.69), channel_id=1, source_target_pairs={{0,12},{1,13},{2,14},{3,15},{4,8},{5,9},{6,10},{7,11},{8,4},{9,5},... | collective-permute-start | bytes 589832 | tf_op jit(solution)/shard_map/ppermute | solution.py:236
  127.1 14.3 %collective-permute-start.36 = (bf16[48,2048]{1,0:T(8,128)(2,1)S(1)}, bf16[48,2048]{1,0:T(8,128)(2,1)S(1)}, u32[]{:S(2)}, u32[]{:S(2)}) collective-permute-start(bf16[48,2048]{1,0:T(8,128)(2,1)S(1)} %get-tuple-element.70), channel_id=1, source_target_pairs={{0,10},{1,11},{2,8},{3,9},{4,14},{5,15},{6,12},{7,13},{8,2},{9,3},... | collective-permute-start | bytes 589832 | tf_op jit(solution)/shard_map/ppermute | solution.py:236
  127.6 15.5 %collective-permute-start.37 = (bf16[48,2048]{1,0:T(8,128)(2,1)S(1)}, bf16[48,2048]{1,0:T(8,128)(2,1)S(1)}, u32[]{:S(2)}, u32[]{:S(2)}) collective-permute-start(bf16[48,2048]{1,0:T(8,128)(2,1)S(1)} %get-tuple-element.71), channel_id=1, source_target_pairs={{0,8},{1,9},{2,10},{3,11},{4,12},{5,13},{6,14},{7,15},{8,0},{9,1},... | collective-permute-start | bytes 589832 | tf_op jit(solution)/shard_map/ppermute | solution.py:236
  129.3 13.8 %collective-permute-start.38 = (bf16[48,2048]{1,0:T(8,128)(2,1)S(1)}, bf16[48,2048]{1,0:T(8,128)(2,1)S(1)}, u32[]{:S(2)}, u32[]{:S(2)}) collective-permute-start(bf16[48,2048]{1,0:T(8,128)(2,1)S(1)} %get-tuple-element.72), channel_id=1, source_target_pairs={{0,6},{1,7},{2,4},{3,5},{4,2},{5,3},{6,0},{7,1},{8,14},{9,15},{10,... | collective-permute-start | bytes 589832 | tf_op jit(solution)/shard_map/ppermute | solution.py:236
  145.8 24.7 %collective-permute-start.41 = (bf16[128,2048]{1,0:T(8,128)(2,1)S(1)}, bf16[128,2048]{1,0:T(8,128)(2,1)S(1)}, u32[]{:S(2)}, u32[]{:S(2)}) collective-permute-start(bf16[128,2048]{1,0:T(8,128)(2,1)S(1)} %get-tuple-element.76), channel_id=1, source_target_pairs={{0,1},{1,0},{2,3},{3,2},{4,5},{5,4},{6,7},{7,6},{8,9},{9,8},{10,11... | collective-permute-start | bytes 1572872 | tf_op jit(solution)/shard_map/ppermute | solution.py:236
  146.8 13.7 %collective-permute-start.20 = (bf16[48,2048]{1,0:T(8,128)(2,1)S(1)}, bf16[48,2048]{1,0:T(8,128)(2,1)S(1)}, u32[]{:S(2)}, u32[]{:S(2)}) collective-permute-start(bf16[48,2048]{1,0:T(8,128)(2,1)S(1)} %get-tuple-element.52), channel_id=1, source_target_pairs={{0,12},{1,13},{2,14},{3,15},{4,8},{5,9},{6,10},{7,11},{8,4},{9,5},... | collective-permute-start | bytes 589832 | tf_op jit(solution)/shard_map/ppermute | solution.py:236
  149.7 13.6 %collective-permute-start.21 = (bf16[48,2048]{1,0:T(8,128)(2,1)S(1)}, bf16[48,2048]{1,0:T(8,128)(2,1)S(1)}, u32[]{:S(2)}, u32[]{:S(2)}) collective-permute-start(bf16[48,2048]{1,0:T(8,128)(2,1)S(1)} %get-tuple-element.53), channel_id=1, source_target_pairs={{0,10},{1,11},{2,8},{3,9},{4,14},{5,15},{6,12},{7,13},{8,2},{9,3},... | collective-permute-start | bytes 589832 | tf_op jit(solution)/shard_map/ppermute | solution.py:236
  149.7 16.5 %collective-permute-start.22 = (bf16[48,2048]{1,0:T(8,128)(2,1)S(1)}, bf16[48,2048]{1,0:T(8,128)(2,1)S(1)}, u32[]{:S(2)}, u32[]{:S(2)}) collective-permute-start(bf16[48,2048]{1,0:T(8,128)(2,1)S(1)} %get-tuple-element.54), channel_id=1, source_target_pairs={{0,8},{1,9},{2,10},{3,11},{4,12},{5,13},{6,14},{7,15},{8,0},{9,1},... | collective-permute-start | bytes 589832 | tf_op jit(solution)/shard_map/ppermute | solution.py:236
  155.6 11.5 %collective-permute-start.23 = (bf16[48,2048]{1,0:T(8,128)(2,1)S(1)}, bf16[48,2048]{1,0:T(8,128)(2,1)S(1)}, u32[]{:S(2)}, u32[]{:S(2)}) collective-permute-start(bf16[48,2048]{1,0:T(8,128)(2,1)S(1)} %get-tuple-element.55), channel_id=1, source_target_pairs={{0,6},{1,7},{2,4},{3,5},{4,2},{5,3},{6,0},{7,1},{8,14},{9,15},{10,... | collective-permute-start | bytes 589832 | tf_op jit(solution)/shard_map/ppermute | solution.py:236
  170.6 26.5 %collective-permute-start.42 = (bf16[128,2048]{1,0:T(8,128)(2,1)S(1)}, bf16[128,2048]{1,0:T(8,128)(2,1)S(1)}, u32[]{:S(2)}, u32[]{:S(2)}) collective-permute-start(bf16[128,2048]{1,0:T(8,128)(2,1)S(1)} %add_convert_fusion), channel_id=1, source_target_pairs={{0,16},{1,17},{2,18},{3,19},{4,20},{5,21},{6,22},{7,23},{8,24},{9,... | collective-permute-start | bytes 1572872 | tf_op jit(solution)/shard_map/ppermute | solution.py:236
  (40 other events, 601.8 us)
where the time goes:
time: 199 us; the launch traced here: 198 us
  waiting for transfers between devices  108 us (54%)
  starting transfers between devices  48.6 us (24%)
  Pallas kernels  29.6 us (15%)
  local copies, waits for them, and re-layouts  10.4 us (5%)
    ppermute x43, waiting for transfers between devices, send(): return lax.ppermute(values, ('sp', 'dp'), pairs)  108 us
    ppermute x43, starting transfers between devices, send(): return lax.ppermute(values, ('sp', 'dp'), pairs)  48.6 us
    pallas_call x1, Pallas kernels, attention_layer(): pl.pallas_call(functools.partial(attention_kernel, blocks, len(after), la...  14.2 us
    pallas_call x3, Pallas kernels, swiglu(): pl.pallas_call(functools.partial(swiglu_kernel, count, len(after), scale)...  9.62 us
    unnamed x46, local copies, waits for them, and re-layouts  7.27 us
  transfers between devices with their start and end apart: 43, of which 26 were waited for; matrix products, arithmetic and copies ran while one was open for 3% of the time, Pallas kernels for 4%

commit v1 on v0

--- a/solution.py
+++ b/solution.py
@@ -184,7 +184,7 @@
 def swiglu(parts, gate_mat, up_mat, down_mat, kind, after=(), scale=0.0):
     count, (size, width) = len(parts), parts[0].shape
     hidden = gate_mat.shape[-1]
-    block = min(hidden, 256)
+    block = hidden
     lead = (None,) * (gate_mat.ndim - 2)
     zero = (0,) * len(lead)
     whole = pl.BlockSpec((size, width), lambda i: (0, 0))
@@ -473,7 +473,10 @@
     )
 
     def exchange(parts):
-        return [parts[0]] + [send(parts[o], *offsets[o]) for o in range(1, peers)]
+        outs = [parts[0]]
+        for o in range(1, peers):
+            outs.append(send(parts[o], *offsets[o]))
+        return outs
 
     experts = functools.partial(swiglu, gate_mat=gate_proj, up_mat=up_proj, down_mat=down_proj)
     far = send(first, half, 0)

time: 199 us -> 196 us (0.985)
  Pallas kernels: 29.6 us -> 26.2 us
    pallas_call x3, Pallas kernels: 9.62 us -> 6.42 us  [swiglu(): pl.pallas_call(functools.partial(swiglu_kernel, count, len(after), scale)...]
  transfers between devices with their start and end apart: 43 -> 43, of which waited for: 26 -> 26; matrix products, arithmetic and copies ran while one was open for 3% -> 3% of each run, Pallas kernels for 4% -> 3%
where the time goes in v1:
time: 196 us
  waiting for transfers between devices  107 us (55%)
  starting transfers between devices  48.8 us (25%)
  Pallas kernels  26.2 us (13%)
  local copies, waits for them, and re-layouts  11.3 us (6%)
    ppermute x43, waiting for transfers between devices, send(): return lax.ppermute(values, ('sp', 'dp'), pairs)  107 us
    ppermute x43, starting transfers between devices, send(): return lax.ppermute(values, ('sp', 'dp'), pairs)  48.8 us
    pallas_call x1, Pallas kernels, attention_layer(): pl.pallas_call(functools.partial(attention_kernel, blocks, len(after), la...  14 us
    unnamed x46, local copies, waits for them, and re-layouts  8.13 us
    pallas_call x3, Pallas kernels, swiglu(): pl.pallas_call(functools.partial(swiglu_kernel, count, len(after), scale)...  6.42 us
  transfers between devices with their start and end apart: 43, of which 26 were waited for; matrix products, arithmetic and copies ran while one was open for 3% of the time, Pallas kernels for 3%

profile of v1, /device:TPU:0, one launch (start us, length us, event | category | flops | bytes accessed | tf_op | source)
XLA Modules:
  0.0 195.8 jit_solution(2418937681634169891)
XLA Ops:
  1.9 4.1 %collective-permute-start.3 = (bf16[128,640]{1,0:T(8,128)(2,1)}, bf16[128,640]{1,0:T(8,128)(2,1)S(1)}, u32[]{:S(2)}, u32[]{:S(2)}) collective-permute-start(bf16[128,640]{1,0:T(8,128)(2,1)} %pack.1.refs_0_), channel_id=1, source_target_pairs={{0,16},{1,17},{2,18},{3,19},{4,20},{5,21},{6,22},{7,23},{8,24},{9,... | collective-permute-start | bytes 491528 | tf_op jit(solution)/shard_map/ppermute | solution.py:236
  11.4 4.1 %collective-permute-done.3.refs_4_ = bf16[128,640]{1,0:T(8,128)(2,1)S(1)} collective-permute-done((bf16[128,640]{1,0:T(8,128)(2,1)}, bf16[128,640]{1,0:T(8,128)(2,1)S(1)}, u32[]{:S(2)}, u32[]{:S(2)}) %collective-permute-start.3) | collective-permute-done | bytes 163872 | tf_op jit(solution)/shard_map/ppermute | solution.py:236
  15.7 2.1 %collective-permute-start.4 = (bf16[128,640]{1,0:T(8,128)(2,1)S(1)}, bf16[128,640]{1,0:T(8,128)(2,1)S(1)}, u32[]{:S(2)}, u32[]{:S(2)}) collective-permute-start(bf16[128,640]{1,0:T(8,128)(2,1)S(1)} %collective-permute-done.3.refs_4_), channel_id=1, source_target_pairs={{0,4},{1,5},{2,6},{3,7},{4,0},{5,1},{6,2},{7,3},{8,12},{9,13},{10,... | collective-permute-start | bytes 491528 | tf_op jit(solution)/shard_map/ppermute | solution.py:236
  26.4 3.3 %collective-permute-done.6.refs_7_ = bf16[128,640]{1,0:T(8,128)(2,1)S(1)} collective-permute-done((bf16[128,640]{1,0:T(8,128)(2,1)S(1)}, bf16[128,640]{1,0:T(8,128)(2,1)S(1)}, u32[]{:S(2)}, u32[]{:S(2)}) %collective-permute-start.6) | collective-permute-done | bytes 163872 | tf_op jit(solution)/shard_map/ppermute | solution.py:236
  30.4 14.0 %attention_layer.1.own_ref.refs_0_ = bf16[128,2048]{1,0:T(8,128)(2,1)} custom-call(s32[1]{0:T(128)} %bitcast.here_ref, bf16[128,1536]{1,0:T(8,128)(2,1)} %bitcast.83, f32[1024,128]{1,0:T(8,128)} %constant.23.clone.table_ref, bf16[128,640]{1,0:T(8,128)(2,1)} %pack.1.refs_0_, bf16[128,640]{1,0:T(8,128)(2,1)} %copy-done.17, bf16[128,640]{1,0:T(8,128)(2,1)} %copy-done.15, ...), custom_call_target="tpu_custom_call" | custom-call | tf_op jit(solution)/shard_map/attention_layer/pallas_call | solution.py:332
  45.1 25.3 %collective-permute-done.17.own_ref = bf16[128,2048]{1,0:T(8,128)(2,1)S(1)} collective-permute-done((bf16[128,2048]{1,0:T(8,128)(2,1)}, bf16[128,2048]{1,0:T(8,128)(2,1)S(1)}, u32[]{:S(2)}, u32[]{:S(2)}) %collective-permute-start.17) | collective-permute-done | bytes 524320 | tf_op jit(solution)/shard_map/ppermute | solution.py:236
  72.6 3.4 %collective-permute-start.11 = (bf16[48,2048]{1,0:T(8,128)(2,1)S(1)}, bf16[48,2048]{1,0:T(8,128)(2,1)S(1)}, u32[]{:S(2)}, u32[]{:S(2)}) collective-permute-start(bf16[48,2048]{1,0:T(8,128)(2,1)S(1)} %get-tuple-element.43), channel_id=1, source_target_pairs={{0,12},{1,13},{2,14},{3,15},{4,8},{5,9},{6,10},{7,11},{8,4},{9,5},... | collective-permute-start | bytes 589832 | tf_op jit(solution)/shard_map/ppermute | solution.py:236
  78.0 2.5 %collective-permute-start.14 = (bf16[48,2048]{1,0:T(8,128)(2,1)S(1)}, bf16[48,2048]{1,0:T(8,128)(2,1)S(1)}, u32[]{:S(2)}, u32[]{:S(2)}) collective-permute-start(bf16[48,2048]{1,0:T(8,128)(2,1)S(1)} %get-tuple-element.46), channel_id=1, source_target_pairs={{0,6},{1,7},{2,4},{3,5},{4,2},{5,3},{6,0},{7,1},{8,14},{9,15},{10,... | collective-permute-start | bytes 589832 | tf_op jit(solution)/shard_map/ppermute | solution.py:236
  83.6 6.0 %collective-permute-done.11.refs_2_ = bf16[48,2048]{1,0:T(8,128)(2,1)S(1)} collective-permute-done((bf16[48,2048]{1,0:T(8,128)(2,1)S(1)}, bf16[48,2048]{1,0:T(8,128)(2,1)S(1)}, u32[]{:S(2)}, u32[]{:S(2)}) %collective-permute-start.11) | collective-permute-done | bytes 196640 | tf_op jit(solution)/shard_map/ppermute | solution.py:236
  90.2 2.7 %collective-permute-done.12.refs_3_ = bf16[48,2048]{1,0:T(8,128)(2,1)S(1)} collective-permute-done((bf16[48,2048]{1,0:T(8,128)(2,1)S(1)}, bf16[48,2048]{1,0:T(8,128)(2,1)S(1)}, u32[]{:S(2)}, u32[]{:S(2)}) %collective-permute-start.12) | collective-permute-done | bytes 196640 | tf_op jit(solution)/shard_map/ppermute | solution.py:236
  93.3 3.9 %collective-permute-done.13.refs_4_ = bf16[48,2048]{1,0:T(8,128)(2,1)S(1)} collective-permute-done((bf16[48,2048]{1,0:T(8,128)(2,1)S(1)}, bf16[48,2048]{1,0:T(8,128)(2,1)S(1)}, u32[]{:S(2)}, u32[]{:S(2)}) %collective-permute-start.13) | collective-permute-done | bytes 196640 | tf_op jit(solution)/shard_map/ppermute | solution.py:236
  104.2 4.4 %collective-permute-done.28.refs_2_ = bf16[48,2048]{1,0:T(8,128)(2,1)S(1)} collective-permute-done((bf16[48,2048]{1,0:T(8,128)(2,1)S(1)}, bf16[48,2048]{1,0:T(8,128)(2,1)S(1)}, u32[]{:S(2)}, u32[]{:S(2)}) %collective-permute-start.28) | collective-permute-done | bytes 196640 | tf_op jit(solution)/shard_map/ppermute | solution.py:236
  115.4 2.7 %swiglu.4 = (bf16[48,2048]{1,0:T(8,128)(2,1)S(1)}, bf16[48,2048]{1,0:T(8,128)(2,1)S(1)}, bf16[48,2048]{1,0:T(8,128)(2,1)S(1)}, bf16[48,2048]{1,0:T(8,128)(2,1)S(...) custom-call(bf16[48,2048]{1,0:T(8,128)(2,1)S(1)} %get-tuple-element., ...), custom_call_target="tpu_custom_call" | custom-call | tf_op jit(solution)/shard_map/swiglu/pallas_call | solution.py:191
  118.2 2.7 %swiglu.5 = (bf16[48,2048]{1,0:T(8,128)(2,1)S(1)}, bf16[48,2048]{1,0:T(8,128)(2,1)S(1)}, bf16[48,2048]{1,0:T(8,128)(2,1)S(1)}, bf16[48,2048]{1,0:T(8,128)(2,1)S(...) custom-call(bf16[48,2048]{1,0:T(8,128)(2,1)S(1)} %get-tuple-element., ...), custom_call_target="tpu_custom_call" | custom-call | tf_op jit(solution)/shard_map/swiglu/pallas_call | solution.py:191
  120.9 3.6 %collective-permute-start.35 = (bf16[48,2048]{1,0:T(8,128)(2,1)S(1)}, bf16[48,2048]{1,0:T(8,128)(2,1)S(1)}, u32[]{:S(2)}, u32[]{:S(2)}) collective-permute-start(bf16[48,2048]{1,0:T(8,128)(2,1)S(1)} %get-tuple-element.69), channel_id=1, source_target_pairs={{0,12},{1,13},{2,14},{3,15},{4,8},{5,9},{6,10},{7,11},{8,4},{9,5},... | collective-permute-start | bytes 589832 | tf_op jit(solution)/shard_map/ppermute | solution.py:236
  126.7 2.6 %collective-permute-start.38 = (bf16[48,2048]{1,0:T(8,128)(2,1)S(1)}, bf16[48,2048]{1,0:T(8,128)(2,1)S(1)}, u32[]{:S(2)}, u32[]{:S(2)}) collective-permute-start(bf16[48,2048]{1,0:T(8,128)(2,1)S(1)} %get-tuple-element.72), channel_id=1, source_target_pairs={{0,6},{1,7},{2,4},{3,5},{4,2},{5,3},{6,0},{7,1},{8,14},{9,15},{10,... | collective-permute-start | bytes 589832 | tf_op jit(solution)/shard_map/ppermute | solution.py:236
  132.5 2.6 %collective-permute-done.35.refs_2_ = bf16[48,2048]{1,0:T(8,128)(2,1)S(1)} collective-permute-done((bf16[48,2048]{1,0:T(8,128)(2,1)S(1)}, bf16[48,2048]{1,0:T(8,128)(2,1)S(1)}, u32[]{:S(2)}, u32[]{:S(2)}) %collective-permute-start.35) | collective-permute-done | bytes 196640 | tf_op jit(solution)/shard_map/ppermute | solution.py:236
  135.8 3.1 %collective-permute-done.36.refs_3_ = bf16[48,2048]{1,0:T(8,128)(2,1)S(1)} collective-permute-done((bf16[48,2048]{1,0:T(8,128)(2,1)S(1)}, bf16[48,2048]{1,0:T(8,128)(2,1)S(1)}, u32[]{:S(2)}, u32[]{:S(2)}) %collective-permute-start.36) | collective-permute-done | bytes 196640 | tf_op jit(solution)/shard_map/ppermute | solution.py:236
  144.3 2.9 %collective-permute-start.20 = (bf16[48,2048]{1,0:T(8,128)(2,1)S(1)}, bf16[48,2048]{1,0:T(8,128)(2,1)S(1)}, u32[]{:S(2)}, u32[]{:S(2)}) collective-permute-start(bf16[48,2048]{1,0:T(8,128)(2,1)S(1)} %get-tuple-element.52), channel_id=1, source_target_pairs={{0,12},{1,13},{2,14},{3,15},{4,8},{5,9},{6,10},{7,11},{8,4},{9,5},... | collective-permute-start | bytes 589832 | tf_op jit(solution)/shard_map/ppermute | solution.py:236
  149.3 3.8 %collective-permute-done.19.refs_1_ = bf16[48,2048]{1,0:T(8,128)(2,1)S(1)} collective-permute-done((bf16[48,2048]{1,0:T(8,128)(2,1)S(1)}, bf16[48,2048]{1,0:T(8,128)(2,1)S(1)}, u32[]{:S(2)}, u32[]{:S(2)}) %collective-permute-start.19) | collective-permute-done | bytes 196640 | tf_op jit(solution)/shard_map/ppermute | solution.py:236
  154.3 3.6 %collective-permute-done.20.refs_2_ = bf16[48,2048]{1,0:T(8,128)(2,1)S(1)} collective-permute-done((bf16[48,2048]{1,0:T(8,128)(2,1)S(1)}, bf16[48,2048]{1,0:T(8,128)(2,1)S(1)}, u32[]{:S(2)}, u32[]{:S(2)}) %collective-permute-start.20) | collective-permute-done | bytes 196640 | tf_op jit(solution)/shard_map/ppermute | solution.py:236
  158.0 2.7 %collective-permute-done.21.refs_3_ = bf16[48,2048]{1,0:T(8,128)(2,1)S(1)} collective-permute-done((bf16[48,2048]{1,0:T(8,128)(2,1)S(1)}, bf16[48,2048]{1,0:T(8,128)(2,1)S(1)}, u32[]{:S(2)}, u32[]{:S(2)}) %collective-permute-start.21) | collective-permute-done | bytes 196640 | tf_op jit(solution)/shard_map/ppermute | solution.py:236
  161.5 2.2 %collective-permute-done.22.refs_4_ = bf16[48,2048]{1,0:T(8,128)(2,1)S(1)} collective-permute-done((bf16[48,2048]{1,0:T(8,128)(2,1)S(1)}, bf16[48,2048]{1,0:T(8,128)(2,1)S(1)}, u32[]{:S(2)}, u32[]{:S(2)}) %collective-permute-start.22) | collective-permute-done | bytes 196640 | tf_op jit(solution)/shard_map/ppermute | solution.py:236
  169.7 24.7 %collective-permute-done.42.far_ref = bf16[128,2048]{1,0:T(8,128)(2,1)S(1)} collective-permute-done((bf16[128,2048]{1,0:T(8,128)(2,1)S(1)}, bf16[128,2048]{1,0:T(8,128)(2,1)S(1)}, u32[]{:S(2)}, u32[]{:S(2)}) %collective-permute-start.42) | collective-permute-done | bytes 524320 | tf_op jit(solution)/shard_map/ppermute | solution.py:236
  (154 shorter events, 62.5 us)
Async XLA Ops:
  1.9 13.7 %collective-permute-start.3 = (bf16[128,640]{1,0:T(8,128)(2,1)}, bf16[128,640]{1,0:T(8,128)(2,1)S(1)}, u32[]{:S(2)}, u32[]{:S(2)}) collective-permute-start(bf16[128,640]{1,0:T(8,128)(2,1)} %pack.1.refs_0_), channel_id=1, source_target_pairs={{0,16},{1,17},{2,18},{3,19},{4,20},{5,21},{6,22},{7,23},{8,24},{9,... | collective-permute-start | bytes 491528 | tf_op jit(solution)/shard_map/ppermute | solution.py:236
  5.9 12.0 %collective-permute-start.1 = (bf16[128,640]{1,0:T(8,128)(2,1)}, bf16[128,640]{1,0:T(8,128)(2,1)S(1)}, u32[]{:S(2)}, u32[]{:S(2)}) collective-permute-start(bf16[128,640]{1,0:T(8,128)(2,1)} %pack.1.refs_0_), channel_id=1, source_target_pairs={{0,8},{1,9},{2,10},{3,11},{4,12},{5,13},{6,14},{7,15},{8,0},{9,1},... | collective-permute-start | bytes 491528 | tf_op jit(solution)/shard_map/ppermute | solution.py:236
  7.5 17.7 %collective-permute-start = (bf16[128,640]{1,0:T(8,128)(2,1)}, bf16[128,640]{1,0:T(8,128)(2,1)S(1)}, u32[]{:S(2)}, u32[]{:S(2)}) collective-permute-start(bf16[128,640]{1,0:T(8,128)(2,1)} %pack.1.refs_0_), channel_id=1, source_target_pairs={{0,4},{1,5},{2,6},{3,7},{4,0},{5,1},{6,2},{7,3},{8,12},{9,13},{10,... | collective-permute-start | bytes 491528 | tf_op jit(solution)/shard_map/ppermute | solution.py:236
  44.5 26.0 %collective-permute-start.17 = (bf16[128,2048]{1,0:T(8,128)(2,1)}, bf16[128,2048]{1,0:T(8,128)(2,1)S(1)}, u32[]{:S(2)}, u32[]{:S(2)}) collective-permute-start(bf16[128,2048]{1,0:T(8,128)(2,1)} %attention_layer.1.own_ref.refs_0_), channel_id=1, source_target_pairs={{0,16},{1,17},{2,18},{3,19},{4,20},{5,21},{6,22},{7,23},{8,24},{9,... | collective-permute-start | bytes 1572872 | tf_op jit(solution)/shard_map/ppermute | solution.py:236
  45.1 25.3 %collective-permute-start.9 = (bf16[128,2048]{1,0:T(8,128)(2,1)}, bf16[128,2048]{1,0:T(8,128)(2,1)S(1)}, u32[]{:S(2)}, u32[]{:S(2)}) collective-permute-start(bf16[128,2048]{1,0:T(8,128)(2,1)} %attention_layer.1.own_ref.refs_0_), channel_id=1, source_target_pairs={{0,1},{1,0},{2,3},{3,2},{4,5},{5,4},{6,7},{7,6},{8,9},{9,8},{10,11... | collective-permute-start | bytes 1572872 | tf_op jit(solution)/shard_map/ppermute | solution.py:236
  72.6 17.0 %collective-permute-start.11 = (bf16[48,2048]{1,0:T(8,128)(2,1)S(1)}, bf16[48,2048]{1,0:T(8,128)(2,1)S(1)}, u32[]{:S(2)}, u32[]{:S(2)}) collective-permute-start(bf16[48,2048]{1,0:T(8,128)(2,1)S(1)} %get-tuple-element.43), channel_id=1, source_target_pairs={{0,12},{1,13},{2,14},{3,15},{4,8},{5,9},{6,10},{7,11},{8,4},{9,5},... | collective-permute-start | bytes 589832 | tf_op jit(solution)/shard_map/ppermute | solution.py:236
  76.0 17.0 %collective-permute-start.12 = (bf16[48,2048]{1,0:T(8,128)(2,1)S(1)}, bf16[48,2048]{1,0:T(8,128)(2,1)S(1)}, u32[]{:S(2)}, u32[]{:S(2)}) collective-permute-start(bf16[48,2048]{1,0:T(8,128)(2,1)S(1)} %get-tuple-element.44), channel_id=1, source_target_pairs={{0,10},{1,11},{2,8},{3,9},{4,14},{5,15},{6,12},{7,13},{8,2},{9,3},... | collective-permute-start | bytes 589832 | tf_op jit(solution)/shard_map/ppermute | solution.py:236
  76.1 21.1 %collective-permute-start.13 = (bf16[48,2048]{1,0:T(8,128)(2,1)S(1)}, bf16[48,2048]{1,0:T(8,128)(2,1)S(1)}, u32[]{:S(2)}, u32[]{:S(2)}) collective-permute-start(bf16[48,2048]{1,0:T(8,128)(2,1)S(1)} %get-tuple-element.45), channel_id=1, source_target_pairs={{0,8},{1,9},{2,10},{3,11},{4,12},{5,13},{6,14},{7,15},{8,0},{9,1},... | collective-permute-start | bytes 589832 | tf_op jit(solution)/shard_map/ppermute | solution.py:236
  78.0 19.2 %collective-permute-start.14 = (bf16[48,2048]{1,0:T(8,128)(2,1)S(1)}, bf16[48,2048]{1,0:T(8,128)(2,1)S(1)}, u32[]{:S(2)}, u32[]{:S(2)}) collective-permute-start(bf16[48,2048]{1,0:T(8,128)(2,1)S(1)} %get-tuple-element.46), channel_id=1, source_target_pairs={{0,6},{1,7},{2,4},{3,5},{4,2},{5,3},{6,0},{7,1},{8,14},{9,15},{10,... | collective-permute-start | bytes 589832 | tf_op jit(solution)/shard_map/ppermute | solution.py:236
  82.1 16.7 %collective-permute-start.15 = (bf16[48,2048]{1,0:T(8,128)(2,1)S(1)}, bf16[48,2048]{1,0:T(8,128)(2,1)S(1)}, u32[]{:S(2)}, u32[]{:S(2)}) collective-permute-start(bf16[48,2048]{1,0:T(8,128)(2,1)S(1)} %get-tuple-element.47), channel_id=1, source_target_pairs={{0,4},{1,5},{2,6},{3,7},{4,0},{5,1},{6,2},{7,3},{8,12},{9,13},{10,... | collective-permute-start | bytes 589832 | tf_op jit(solution)/shard_map/ppermute | solution.py:236
  97.2 20.9 %collective-permute-start.29 = (bf16[48,2048]{1,0:T(8,128)(2,1)S(1)}, bf16[48,2048]{1,0:T(8,128)(2,1)S(1)}, u32[]{:S(2)}, u32[]{:S(2)}) collective-permute-start(bf16[48,2048]{1,0:T(8,128)(2,1)S(1)} %get-tuple-element.62), channel_id=1, source_target_pairs={{0,10},{1,11},{2,8},{3,9},{4,14},{5,15},{6,12},{7,13},{8,2},{9,3},... | collective-permute-start | bytes 589832 | tf_op jit(solution)/shard_map/ppermute | solution.py:236
  98.8 19.3 %collective-permute-start.30 = (bf16[48,2048]{1,0:T(8,128)(2,1)S(1)}, bf16[48,2048]{1,0:T(8,128)(2,1)S(1)}, u32[]{:S(2)}, u32[]{:S(2)}) collective-permute-start(bf16[48,2048]{1,0:T(8,128)(2,1)S(1)} %get-tuple-element.63), channel_id=1, source_target_pairs={{0,8},{1,9},{2,10},{3,11},{4,12},{5,13},{6,14},{7,15},{8,0},{9,1},... | collective-permute-start | bytes 589832 | tf_op jit(solution)/shard_map/ppermute | solution.py:236
  100.5 17.6 %collective-permute-start.31 = (bf16[48,2048]{1,0:T(8,128)(2,1)S(1)}, bf16[48,2048]{1,0:T(8,128)(2,1)S(1)}, u32[]{:S(2)}, u32[]{:S(2)}) collective-permute-start(bf16[48,2048]{1,0:T(8,128)(2,1)S(1)} %get-tuple-element.64), channel_id=1, source_target_pairs={{0,6},{1,7},{2,4},{3,5},{4,2},{5,3},{6,0},{7,1},{8,14},{9,15},{10,... | collective-permute-start | bytes 589832 | tf_op jit(solution)/shard_map/ppermute | solution.py:236
  102.3 15.8 %collective-permute-start.32 = (bf16[48,2048]{1,0:T(8,128)(2,1)S(1)}, bf16[48,2048]{1,0:T(8,128)(2,1)S(1)}, u32[]{:S(2)}, u32[]{:S(2)}) collective-permute-start(bf16[48,2048]{1,0:T(8,128)(2,1)S(1)} %get-tuple-element.65), channel_id=1, source_target_pairs={{0,4},{1,5},{2,6},{3,7},{4,0},{5,1},{6,2},{7,3},{8,12},{9,13},{10,... | collective-permute-start | bytes 589832 | tf_op jit(solution)/shard_map/ppermute | solution.py:236
  120.9 14.2 %collective-permute-start.35 = (bf16[48,2048]{1,0:T(8,128)(2,1)S(1)}, bf16[48,2048]{1,0:T(8,128)(2,1)S(1)}, u32[]{:S(2)}, u32[]{:S(2)}) collective-permute-start(bf16[48,2048]{1,0:T(8,128)(2,1)S(1)} %get-tuple-element.69), channel_id=1, source_target_pairs={{0,12},{1,13},{2,14},{3,15},{4,8},{5,9},{6,10},{7,11},{8,4},{9,5},... | collective-permute-start | bytes 589832 | tf_op jit(solution)/shard_map/ppermute | solution.py:236
  124.5 14.3 %collective-permute-start.36 = (bf16[48,2048]{1,0:T(8,128)(2,1)S(1)}, bf16[48,2048]{1,0:T(8,128)(2,1)S(1)}, u32[]{:S(2)}, u32[]{:S(2)}) collective-permute-start(bf16[48,2048]{1,0:T(8,128)(2,1)S(1)} %get-tuple-element.70), channel_id=1, source_target_pairs={{0,10},{1,11},{2,8},{3,9},{4,14},{5,15},{6,12},{7,13},{8,2},{9,3},... | collective-permute-start | bytes 589832 | tf_op jit(solution)/shard_map/ppermute | solution.py:236
  125.1 15.5 %collective-permute-start.37 = (bf16[48,2048]{1,0:T(8,128)(2,1)S(1)}, bf16[48,2048]{1,0:T(8,128)(2,1)S(1)}, u32[]{:S(2)}, u32[]{:S(2)}) collective-permute-start(bf16[48,2048]{1,0:T(8,128)(2,1)S(1)} %get-tuple-element.71), channel_id=1, source_target_pairs={{0,8},{1,9},{2,10},{3,11},{4,12},{5,13},{6,14},{7,15},{8,0},{9,1},... | collective-permute-start | bytes 589832 | tf_op jit(solution)/shard_map/ppermute | solution.py:236
  126.7 13.8 %collective-permute-start.38 = (bf16[48,2048]{1,0:T(8,128)(2,1)S(1)}, bf16[48,2048]{1,0:T(8,128)(2,1)S(1)}, u32[]{:S(2)}, u32[]{:S(2)}) collective-permute-start(bf16[48,2048]{1,0:T(8,128)(2,1)S(1)} %get-tuple-element.72), channel_id=1, source_target_pairs={{0,6},{1,7},{2,4},{3,5},{4,2},{5,3},{6,0},{7,1},{8,14},{9,15},{10,... | collective-permute-start | bytes 589832 | tf_op jit(solution)/shard_map/ppermute | solution.py:236
  143.3 24.6 %collective-permute-start.41 = (bf16[128,2048]{1,0:T(8,128)(2,1)S(1)}, bf16[128,2048]{1,0:T(8,128)(2,1)S(1)}, u32[]{:S(2)}, u32[]{:S(2)}) collective-permute-start(bf16[128,2048]{1,0:T(8,128)(2,1)S(1)} %get-tuple-element.76), channel_id=1, source_target_pairs={{0,1},{1,0},{2,3},{3,2},{4,5},{5,4},{6,7},{7,6},{8,9},{9,8},{10,11... | collective-permute-start | bytes 1572872 | tf_op jit(solution)/shard_map/ppermute | solution.py:236
  144.3 13.7 %collective-permute-start.20 = (bf16[48,2048]{1,0:T(8,128)(2,1)S(1)}, bf16[48,2048]{1,0:T(8,128)(2,1)S(1)}, u32[]{:S(2)}, u32[]{:S(2)}) collective-permute-start(bf16[48,2048]{1,0:T(8,128)(2,1)S(1)} %get-tuple-element.52), channel_id=1, source_target_pairs={{0,12},{1,13},{2,14},{3,15},{4,8},{5,9},{6,10},{7,11},{8,4},{9,5},... | collective-permute-start | bytes 589832 | tf_op jit(solution)/shard_map/ppermute | solution.py:236
  147.1 13.5 %collective-permute-start.21 = (bf16[48,2048]{1,0:T(8,128)(2,1)S(1)}, bf16[48,2048]{1,0:T(8,128)(2,1)S(1)}, u32[]{:S(2)}, u32[]{:S(2)}) collective-permute-start(bf16[48,2048]{1,0:T(8,128)(2,1)S(1)} %get-tuple-element.53), channel_id=1, source_target_pairs={{0,10},{1,11},{2,8},{3,9},{4,14},{5,15},{6,12},{7,13},{8,2},{9,3},... | collective-permute-start | bytes 589832 | tf_op jit(solution)/shard_map/ppermute | solution.py:236
  147.2 16.6 %collective-permute-start.22 = (bf16[48,2048]{1,0:T(8,128)(2,1)S(1)}, bf16[48,2048]{1,0:T(8,128)(2,1)S(1)}, u32[]{:S(2)}, u32[]{:S(2)}) collective-permute-start(bf16[48,2048]{1,0:T(8,128)(2,1)S(1)} %get-tuple-element.54), channel_id=1, source_target_pairs={{0,8},{1,9},{2,10},{3,11},{4,12},{5,13},{6,14},{7,15},{8,0},{9,1},... | collective-permute-start | bytes 589832 | tf_op jit(solution)/shard_map/ppermute | solution.py:236
  153.1 11.4 %collective-permute-start.23 = (bf16[48,2048]{1,0:T(8,128)(2,1)S(1)}, bf16[48,2048]{1,0:T(8,128)(2,1)S(1)}, u32[]{:S(2)}, u32[]{:S(2)}) collective-permute-start(bf16[48,2048]{1,0:T(8,128)(2,1)S(1)} %get-tuple-element.55), channel_id=1, source_target_pairs={{0,6},{1,7},{2,4},{3,5},{4,2},{5,3},{6,0},{7,1},{8,14},{9,15},{10,... | collective-permute-start | bytes 589832 | tf_op jit(solution)/shard_map/ppermute | solution.py:236
  168.0 26.5 %collective-permute-start.42 = (bf16[128,2048]{1,0:T(8,128)(2,1)S(1)}, bf16[128,2048]{1,0:T(8,128)(2,1)S(1)}, u32[]{:S(2)}, u32[]{:S(2)}) collective-permute-start(bf16[128,2048]{1,0:T(8,128)(2,1)S(1)} %add_convert_fusion), channel_id=1, source_target_pairs={{0,16},{1,17},{2,18},{3,19},{4,20},{5,21},{6,22},{7,23},{8,24},{9,... | collective-permute-start | bytes 1572872 | tf_op jit(solution)/shard_map/ppermute | solution.py:236
  (40 other events, 597.4 us)
